TPU v7x, 32 devices: a whole 2x2x4 slice. The times are simulated.
32 devices in a mesh: sp: 8 (over z, x), dp: 4 (over y, core).
Axes of the slice: x: 2, y: 2, z: 4, core: 2. Of those that a mesh axis runs over, the one named last changes fastest.
Arguments:
- tokens: bfloat16 [4, 4096, 4096], P('dp', 'sp'), may hold values from -6 to 6
- documents: int32 [4, 4096], P('dp', 'sp'), may hold values from 0 to 7, never falling along the last dimension, each value on 1 to 1024 neighbouring positions
- value_weight: bfloat16 [4096, 2048], P(('sp', 'dp')), may hold values from -0.09375 to 0.09375
- gate_weight: bfloat16 [4096, 2048], P(('sp', 'dp')), may hold values from -0.09375 to 0.09375
- conv_weight: bfloat16 [31, 2048], replicated, may hold values from -1 to 1
- norm_gain: float32 [2048], replicated, may hold values from 0.1 to 1.9
- norm_bias: float32 [2048], replicated, may hold values from -2 to 2
Outputs:
- activated: bfloat16 [4, 4096, 2048], P('dp', 'sp')
Inputs may be any that keep to these rules, and one draw needn't show every extreme that they name: `documents`: document numbers never fall along a sequence, run from 0 to 7, and each document covers 1 to 1024 positions.
All inputs are finite; a program needn't handle non-finite values.
Results may differ from a plain program's by a relative error of at most 0.0064.
Values may be sent and summed in bfloat16 or wider, within the bound.
A program may use at most 192 MiB of HBM per device.

v0:
```python
import jax
import jax.numpy as jnp
from jax import lax
from jax.sharding import PartitionSpec as P

KERNEL = 31


def passed_along(block, axis, distance):
    devices = range(lax.axis_size(axis))
    route = [(i - distance, i) for i in devices if i - distance in devices]
    return lax.ppermute(block, axis, route)


def convolve(padded, padded_docs, taps, count):
    lead = taps.shape[0] - 1
    here = padded_docs[:, lead : lead + count]
    total = jnp.zeros((padded.shape[0], count, padded.shape[2]), jnp.float32)
    for lag in range(taps.shape[0]):
        begin = lead - lag
        moved = padded[:, begin : begin + count].astype(jnp.float32)
        keep = (padded_docs[:, begin : begin + count] == here)[:, :, None]
        total = total + jnp.where(keep, moved, 0.0) * taps[lag].astype(jnp.float32)
    return total


def finish(mixed, norm_gain, norm_bias):
    wide = mixed.astype(jnp.float32)
    center = wide - jnp.mean(wide, axis=-1, keepdims=True)
    spread = jnp.mean(center * center, axis=-1, keepdims=True)
    normed = center * lax.rsqrt(spread + 1e-06) * norm_gain + norm_bias
    return jax.nn.silu(normed).astype(jnp.bfloat16)


def gated(value, gate):
    return (value.astype(jnp.float32) * jax.nn.sigmoid(gate.astype(jnp.float32))).astype(
        jnp.bfloat16
    )


def per_device(tokens, documents, value_weight, gate_weight, conv_weight, norm_gain, norm_bias):
    batch, count, width = tokens.shape
    channels = value_weight.shape[1]
    lead = KERNEL - 1
    rows = tokens.reshape(batch * count, width)
    value_sum = jnp.dot(
        rows,
        lax.all_gather(value_weight, ("sp", "dp"), axis=0, tiled=True),
        preferred_element_type=jnp.float32,
    )
    gate_sum = jnp.dot(
        rows,
        lax.all_gather(gate_weight, ("sp", "dp"), axis=0, tiled=True),
        preferred_element_type=jnp.float32,
    )
    value, gate = lax.optimization_barrier(
        (value_sum.astype(jnp.bfloat16), gate_sum.astype(jnp.bfloat16))
    )
    value = value.reshape(batch, count, channels)
    gate = gate.reshape(batch, count, channels)
    glu = lax.optimization_barrier(gated(value, gate))
    doc_marks = documents.astype(jnp.bfloat16)
    tail_rows = glu[:, count - lead :]
    tail_docs = doc_marks[:, count - lead :]
    before_rows, before_docs = passed_along((tail_rows, tail_docs), "sp", 1)
    first_span = lax.axis_index("sp") == 0
    edge_fill = jnp.where(first_span, -1.0, before_docs.astype(jnp.float32))
    docs_wide = jnp.concatenate([edge_fill, doc_marks.astype(jnp.float32)], axis=1)
    extended = jnp.concatenate([before_rows, glu], axis=1)
    mixed = convolve(extended, docs_wide, conv_weight, count).astype(jnp.bfloat16)
    mixed = lax.optimization_barrier(mixed)
    return finish(mixed, norm_gain, norm_bias)


def solution(mesh):
    return jax.shard_map(
        per_device,
        mesh=mesh,
        in_specs=(
            P("dp", "sp", None),
            P("dp", "sp"),
            P(("sp", "dp"), None),
            P(("sp", "dp"), None),
            P(),
            P(),
            P(),
        ),
        out_specs=P("dp", "sp", None),
        check_vma=False,
    )
```

profile of v0, /device:TPU:0, one launch (start us, length us, event | category | flops | bytes accessed | tf_op | source)
XLA Modules:
  0.0 317.8 jit_solution(2966811284700309097)
XLA Ops:
  6.5 0.0 all-gather.3.cloned.1.call-start
  6.5 0.7 all-gather.3.cloned.1.call-update
  7.3 0.0 all-gather.5.cloned.1.call-start
  7.3 0.7 all-gather.5.cloned.1.call-update
  8.0 0.7 convert_convert_fusion
  8.7 0.1 slice.372
  8.8 4.9 %collective-permute-start = (bf16[1,30]{1,0:T(2,128)(2,1)S(1)}, bf16[1,30]{1,0:T(2,128)(2,1)S(1)}, u32[]{:S(2)}, u32[]{:S(2)}) collective-permute-start(bf16[1,30]{1,0:T(2,128)(2,1)S(1)} %slice.372), channel_id=1, source_target_pairs={{0,4},{4,8},{8,12},{12,16},{16,20},{20,24},{24,28},{1,5},{5,9},{9,... | collective-permute-start | bytes 188 | tf_op jit(solution)/shard_map/ppermute | solution.py:12
  13.6 1.2 slice_convert_fusion.29
  14.8 1.4 slice_convert_fusion.30
  16.3 0.0 collective-permute-done
  16.3 0.8 compare_reduce_fusion.29
  17.1 0.8 compare_reduce_fusion.28
  17.9 0.8 compare_reduce_fusion.27
  18.7 0.8 compare_reduce_fusion.26
  19.5 0.8 compare_reduce_fusion.25
  20.3 0.8 compare_reduce_fusion.24
  21.1 106.3 %all-gather.3.cloned.1.call-done = bf16[4096,2048]{1,0:T(8,128)(2,1)} async-done(((bf16[128,2048]{1,0:T(8,128)(2,1)}), bf16[4096,2048]{1,0:T(8,128)(2,1)}) %all-gather.3.cloned.1.call-update) | async-done | bytes 16777232 | tf_op jit(solution)/shard_map/all_gather | solution.py:48
  127.4 13.6 %fusion.15 = bf16[512,2048]{1,0:T(8,128)(2,1)S(1)} fusion(bf16[4096,2048]{1,0:T(8,128)(2,1)} %all-gather.3.cloned.1.call-done, bf16[1,512,4096]{2,1,0:T(8,128)(2,1)} %param.7), kind=kOutput, calls=%fused_computation.48 | convolution fusion | flops 8590983168 | bytes 23068672 | tf_op jit(solution)/shard_map/dot_general | solution.py:46
  141.0 101.9 %all-gather.5.cloned.1.call-done = bf16[4096,2048]{1,0:T(8,128)(2,1)} async-done(((bf16[128,2048]{1,0:T(8,128)(2,1)}), bf16[4096,2048]{1,0:T(8,128)(2,1)}) %all-gather.5.cloned.1.call-update) | async-done | bytes 16777232 | tf_op jit(solution)/shard_map/all_gather | solution.py:53
  242.8 13.6 %fusion.18 = bf16[512,2048]{1,0:T(8,128)(2,1)S(1)} fusion(bf16[4096,2048]{1,0:T(8,128)(2,1)} %all-gather.5.cloned.1.call-done, bf16[1,512,4096]{2,1,0:T(8,128)(2,1)} %param.7), kind=kOutput, calls=%fused_computation.49 | convolution fusion | flops 8590983168 | bytes 23068672 | tf_op jit(solution)/shard_map/dot_general | solution.py:51
  256.4 0.0 copy-start
  256.4 1.2 fusion.50
  257.7 3.3 %collective-permute-start.1 = (bf16[1,30,2048]{2,1,0:T(8,128)(2,1)S(1)}, bf16[1,30,2048]{2,1,0:T(8,128)(2,1)S(1)}, u32[]{:S(2)}, u32[]{:S(2)}) collective-permute-start(bf16[1,30,2048]{2,1,0:T(8,128)(2,1)S(1)} %slice.375), channel_id=1, source_target_pairs={{0,4},{4,8},{8,12},{12,16},{16,20},{20,24},{24,28},{1,5},{5,9},{9,... | collective-permute-start | bytes 368648 | tf_op jit(solution)/shard_map/ppermute | solution.py:12
  261.0 0.0 copy-done
  261.0 0.1 compare_reduce_fusion.22
  261.1 0.1 compare_reduce_fusion.23
  261.2 2.7 collective-permute-done.1
  264.0 0.0 copy-start.1
  264.0 0.0 copy-start.2
  264.0 42.9 %add_convert_fusion = bf16[1,512,2048]{2,1,0:T(8,128)(2,1)S(1)} fusion(bf16[1,512,2048]{2,1,0:T(8,128)(2,1)S(1)} %fusion.50, bf16[1,30,2048]{2,1,0:T(8,128)(2,1)S(1)} %collective-permute-done.1, f32[2048]{0:T(1024)S(1)} %bitcast.54, f32[2048]{0:T(1024)S(1)} %bitcast.55, f32[2048]{0:T(1024)S(1)} %bitcast.57, f32[2048]{0:T(1024)S(1)} %bitcast.58, ...), kind=kLoop, calls=%fused_computation.46 | loop fusion | flops 224395264 | bytes 4587008 | tf_op jit(solution)/shard_map/convert_element_type | solution.py:70
  306.9 0.3 convert_reduce_fusion
  307.2 0.7 fusion.2
  307.9 0.0 copy-done.1
  307.9 0.0 copy-done.2
  307.9 3.0 fusion.10
  (4 shorter events, 0.1 us)
Async XLA Ops:
  6.5 120.8 %all-gather.3.cloned.1.call-start = ((), (), s32[]{:S(2)}) async-start(), calls=%async_computation | async-start | bytes 17301504 | tf_op jit(solution)/shard_map/all_gather | solution.py:48
  7.3 235.6 %all-gather.5.cloned.1.call-start = ((), (), s32[]{:S(2)}) async-start(), calls=%async_computation.1 | async-start | bytes 17301504 | tf_op jit(solution)/shard_map/all_gather | solution.py:53
  8.8 7.5 %collective-permute-start = (bf16[1,30]{1,0:T(2,128)(2,1)S(1)}, bf16[1,30]{1,0:T(2,128)(2,1)S(1)}, u32[]{:S(2)}, u32[]{:S(2)}) collective-permute-start(bf16[1,30]{1,0:T(2,128)(2,1)S(1)} %slice.372), channel_id=1, source_target_pairs={{0,4},{4,8},{8,12},{12,16},{16,20},{20,24},{24,28},{1,5},{5,9},{9,... | collective-permute-start | bytes 188 | tf_op jit(solution)/shard_map/ppermute | solution.py:12
  256.4 4.6 %copy-start = (s32[1,512]{1,0:T(1,128)S(1)}, s32[1,512]{1,0:T(1,128)}, u32[]{:S(2)}) copy-start(s32[1,512]{1,0:T(1,128)} %param.8) | copy-start | bytes 6148
  257.7 6.3 %collective-permute-start.1 = (bf16[1,30,2048]{2,1,0:T(8,128)(2,1)S(1)}, bf16[1,30,2048]{2,1,0:T(8,128)(2,1)S(1)}, u32[]{:S(2)}, u32[]{:S(2)}) collective-permute-start(bf16[1,30,2048]{2,1,0:T(8,128)(2,1)S(1)} %slice.375), channel_id=1, source_target_pairs={{0,4},{4,8},{8,12},{12,16},{16,20},{20,24},{24,28},{1,5},{5,9},{9,... | collective-permute-start | bytes 368648 | tf_op jit(solution)/shard_map/ppermute | solution.py:12
  264.0 43.9 %copy-start.1 = (f32[2048]{0:T(1024)S(1)}, f32[2048]{0:T(1024)}, u32[]{:S(2)}) copy-start(f32[2048]{0:T(1024)} %param.13) | copy-start | bytes 24580
  264.0 44.0 %copy-start.2 = (f32[2048]{0:T(1024)S(1)}, f32[2048]{0:T(1024)}, u32[]{:S(2)}) copy-start(f32[2048]{0:T(1024)} %param.12) | copy-start | bytes 24580
Sparse Core Ops, SparseCore 0:
  10.2 117.1 all-gather.2
  130.2 112.5 all-gather.4
where the time goes:
time: 318 us
  waiting for transfers between devices  212 us (67%)
  other arithmetic  56.4 us (18%)
  matrix products  27.2 us (9%)
  between operations  13.6 us (4%)
  starting transfers between devices  8.24 us (3%)
    all_gather x1, waiting for transfers between devices, per_device(): lax.all_gather(value_weight, ('sp', 'dp'), axis=0, tiled=True)  106 us
    all_gather x1, waiting for transfers between devices, per_device(): lax.all_gather(gate_weight, ('sp', 'dp'), axis=0, tiled=True)  102 us
    convert_element_type x1, other arithmetic, per_device(): convolve(extended, docs_wide, conv_weight, count).astype(jnp.bfloat16)  42.9 us
    dot_general x1, matrix products, per_device(): jnp.dot(rows, lax.all_gather(gate_weight, ('sp', 'dp'), axis=0, tiled=Tru...  13.6 us
    dot_general x1, matrix products, per_device(): jnp.dot(rows, lax.all_gather(value_weight, ('sp', 'dp'), axis=0, tiled=Tr...  13.6 us
    ppermute x2, starting transfers between devices, passed_along(): return lax.ppermute(block, axis, route)  8.2 us
  transfers between devices with their start and end apart: 4, of which 3 were waited for; matrix products, arithmetic and copies ran while one was open for 7% of the time, Pallas kernels for 0%

commit v1 on v0

v1 whole, which is shorter than its diff:
```python
import functools

import jax
import jax.numpy as jnp
from jax import lax
from jax.experimental import pallas as pl
from jax.experimental.pallas import tpu as pltpu
from jax.sharding import PartitionSpec as P

KERNEL = 31
BLOCKS = 4
HALO = 32
MESH = pl.DeviceIdType.MESH


def gather_kernel(
    side, tall, tok_hbm, own_hbm, glu_ref, weights, tok, send, recv, cross, begin, halo
):
    sp, dp = lax.axis_index("sp"), lax.axis_index("dp")
    sp_size = lax.axis_size("sp")
    core, y = lax.rem(dp, 2), lax.div(dp, 2)
    z, x = lax.div(sp, side), lax.rem(sp, side)
    flip = core == 1
    u, v = jnp.where(flip, y, x), jnp.where(flip, x, y)
    half = own_hbm.shape[2]
    depth = 2 * half
    count = tok_hbm.shape[0]
    sub = tall // 2
    columns = weights.shape[3] // sub
    wide = columns // 2
    other = {"sp": sp, "dp": y * 2 + (1 - core)}

    def device(dz, du, dv):
        dx, dy = jnp.where(flip, dv, du), jnp.where(flip, du, dv)
        return {"sp": dz * side + dx, "dp": dy * 2 + core}

    def number(pz, pu, pv):
        px, py = jnp.where(flip, pv, pu), jnp.where(flip, pu, pv)
        return (pz * side + px) * side + py

    def piece(plane, block, q):
        return weights.at[plane, block, pl.ds(pl.multiple_of(q * depth, depth), depth), :]

    def link(kind, block, q, target):
        return pltpu.make_async_remote_copy(
            src_ref=piece(core, block, q),
            dst_ref=piece(core, block, q),
            send_sem=send.at[kind, block, q],
            recv_sem=recv.at[block, q],
            device_id=target,
            device_id_type=MESH,
        )

    def hand_over(plane, block, q):
        return pltpu.make_async_remote_copy(
            src_ref=piece(plane, block, q),
            dst_ref=piece(plane, block, q),
            send_sem=send.at[6, block, q],
            recv_sem=cross.at[block, q],
            device_id=other,
            device_id_type=MESH,
        )

    def routes(block, pz, pu, pv, act):
        q = number(pz, pu, pv)
        tall_first = block == 1
        home_u, home_v, home_z = u == pu, v == pv, z == pz
        along_z = home_v & (home_u | jnp.logical_not(tall_first))
        along_u = home_v & (home_z | tall_first)
        ways = (
            (along_z & (z >= pz) & (z + 1 < tall), (z + 1, u, v)),
            (along_z & (z <= pz) & (z > 0), (z - 1, u, v)),
            (along_u & (u >= pu) & (u + 1 < side), (z, u + 1, v)),
            (along_u & (u <= pu) & (u > 0), (z, u - 1, v)),
            ((v >= pv) & (v + 1 < side), (z, u, v + 1)),
            ((v <= pv) & (v > 0), (z, u, v - 1)),
        )
        for kind, (taken, target) in enumerate(ways):

            @pl.when(taken)
            def _(kind=kind, target=target):
                act(link(kind, block, q, device(*target)))

        @pl.when(jnp.logical_not(home_u & home_v & home_z))
        def _():
            act(hand_over(core, block, q))

    def pass_on(block, pz, pu, pv):
        routes(block, pz, pu, pv, lambda copy: copy.start())

    def arrived(block, pz, pu, pv):
        link(0, block, number(pz, pu, pv), other).wait_recv()
        pass_on(block, pz, pu, pv)

    low = jnp.minimum(z, tall - 1 - z)

    def near(k):
        step = jnp.where(lax.rem(k, 2) == 1, low - lax.div(k + 1, 2), low + lax.div(k, 2))
        at = jnp.where(k <= 2 * low, step, k)
        return jnp.where(z == low, at, tall - 1 - at)

    barrier = pltpu.get_barrier_semaphore()
    greeted = jnp.int32(1)
    pl.semaphore_signal(barrier, inc=1, device_id=other, device_id_type=MESH)
    for there, target in (
        (z + 1 < tall, device(z + 1, u, v)),
        (z > 0, device(z - 1, u, v)),
        (u + 1 < side, device(z, u + 1, v)),
        (u > 0, device(z, u - 1, v)),
        (v + 1 < side, device(z, u, v + 1)),
        (v > 0, device(z, u, v - 1)),
        (sp + 1 < sp_size, {"sp": sp + 1, "dp": dp}),
        (sp > 0, {"sp": sp - 1, "dp": dp}),
    ):
        greeted = greeted + there.astype(jnp.int32)

        @pl.when(there)
        def _(target=target):
            pl.semaphore_signal(barrier, inc=1, device_id=target, device_id_type=MESH)

    pl.semaphore_wait(barrier, greeted)

    here = (z * side + x) * side + y
    own_rows = weights.at[
        :, :, pl.ds(pl.multiple_of(here * depth + core * half, half), half), :
    ]
    to_other = pltpu.make_async_remote_copy(
        src_ref=own_hbm,
        dst_ref=own_rows,
        send_sem=begin.at[0],
        recv_sem=begin.at[1],
        device_id=other,
        device_id_type=MESH,
    )
    to_other.start()
    keep = pltpu.make_async_copy(own_hbm, own_rows, begin.at[2])
    keep.start()
    load = pltpu.make_async_copy(tok_hbm, tok.at[pl.ds(HALO, count), :], begin.at[3])
    load.start()
    tail = pltpu.make_async_remote_copy(
        src_ref=tok_hbm.at[pl.ds(count - HALO, HALO), :],
        dst_ref=tok.at[pl.ds(0, HALO), :],
        send_sem=halo.at[0],
        recv_sem=halo.at[1],
        device_id={"sp": lax.rem(sp + 1, sp_size), "dp": dp},
        device_id_type=MESH,
    )

    @pl.when(sp + 1 < sp_size)
    def _():
        tail.start()

    @pl.when(sp == 0)
    def _():
        tok[pl.ds(0, HALO), :] = jnp.zeros((HALO, tok.shape[1]), tok.dtype)

    keep.wait()
    to_other.wait_recv()
    pass_on(0, z, u, v)
    load.wait()

    @pl.when(sp > 0)
    def _():
        tail.wait_recv()

    def tick(at, carry):
        block, k = lax.div(at, tall), lax.rem(at, tall)

        @pl.when((block < BLOCKS) & (k > 0))
        def _():
            arrived(block, near(k), u, v)

        @pl.when((block + 1 < BLOCKS) & (k == 0))
        def _():
            pass_on(block + 1, z, u, v)

        second = jnp.maximum(at - 1, 0)
        block2, k2 = lax.div(second, tall), lax.rem(second, tall)

        @pl.when((at >= 1) & (block2 < BLOCKS))
        def _():
            @pl.loop(1, side)
            def _(du):
                arrived(block2, near(k2), lax.rem(u + du, side), v)

        third = jnp.maximum(at - 2, 0)
        block3, k3 = lax.div(third, tall), lax.rem(third, tall)

        @pl.when((at >= 2) & (block3 < BLOCKS))
        def _():
            @pl.loop(0, side)
            def _(du):
                @pl.loop(1, side)
                def _(dv):
                    arrived(block3, near(k3), lax.rem(u + du, side), lax.rem(v + dv, side))

        late = jnp.maximum(at - tall - 2, 0)
        block4, k4 = lax.div(late, tall), lax.rem(late, tall)

        @pl.when((at >= tall + 2) & (k4 == 0))
        def _():
            @pl.loop(0, tall * side * side)
            def _(q):
                @pl.when(q != here)
                def _():
                    hand_over(1 - core, block4, q).wait_recv()

        @pl.when(at >= tall + 2)
        def _():
            plane, part = lax.div(k4, sub), lax.rem(k4, sub)
            held = weights[
                plane, block4, :, pl.ds(pl.multiple_of(part * columns, columns), columns)
            ]
            both = jnp.dot(tok[...], held, preferred_element_type=jnp.float32)
            value = both[:, :wide].astype(jnp.bfloat16).astype(jnp.float32)
            gate = both[:, wide:].astype(jnp.bfloat16).astype(jnp.float32)
            first = ((plane * BLOCKS + block4) * sub + part) * wide
            glu_ref[:, pl.ds(pl.multiple_of(first, wide), wide)] = (
                value * jax.nn.sigmoid(gate)
            ).astype(jnp.bfloat16)

        return carry

    lax.fori_loop(0, BLOCKS * tall + tall + 2, tick, 0)

    @pl.loop(0, BLOCKS)
    def _(block):
        @pl.loop(0, tall)
        def _(pz):
            @pl.loop(0, side)
            def _(pu):
                @pl.loop(0, side)
                def _(pv):
                    routes(block, pz, pu, pv, lambda copy: copy.wait_send())

    to_other.wait_send()

    @pl.when(sp + 1 < sp_size)
    def _():
        tail.wait_send()


def gated_product(rows, value_weight, gate_weight):
    side = lax.axis_size("dp") // 2
    tall = lax.axis_size("sp") // side
    count, width = rows.shape
    depth, channels = value_weight.shape
    wide = channels // (BLOCKS * tall)
    cut = (depth, 2, BLOCKS, tall // 2, 1, wide)
    own = jnp.concatenate([value_weight.reshape(cut), gate_weight.reshape(cut)], axis=4)
    own = own.transpose(1, 2, 0, 3, 4, 5).reshape(2, BLOCKS, depth, channels // BLOCKS)
    pieces = tall * side * side
    return pl.pallas_call(
        functools.partial(gather_kernel, side, tall),
        out_shape=jax.ShapeDtypeStruct((HALO + count, channels), jnp.bfloat16),
        in_specs=[pl.BlockSpec(memory_space=pl.ANY)] * 2,
        out_specs=pl.BlockSpec(memory_space=pltpu.VMEM),
        scratch_shapes=[
            pltpu.VMEM((2, BLOCKS, width, channels // BLOCKS), jnp.bfloat16),
            pltpu.VMEM((HALO + count, width), jnp.bfloat16),
            pltpu.SemaphoreType.DMA((7, BLOCKS, pieces)),
            pltpu.SemaphoreType.DMA((BLOCKS, pieces)),
            pltpu.SemaphoreType.DMA((BLOCKS, pieces)),
            pltpu.SemaphoreType.DMA((4,)),
            pltpu.SemaphoreType.DMA((2,)),
        ],
        compiler_params=pltpu.CompilerParams(
            collective_id=0, has_side_effects=True, vmem_limit_bytes=56 * 1024 * 1024
        ),
    )(rows, own)


def passed_along(block, axis, distance):
    devices = range(lax.axis_size(axis))
    route = [(i - distance, i) for i in devices if i - distance in devices]
    return lax.ppermute(block, axis, route)


def mix_kernel(glu_ref, reach_ref, taps_ref, gain_ref, bias_ref, out_ref, mixed):
    rows, channels = out_ref.shape
    top = pl.multiple_of(pl.program_id(0) * rows, rows)
    reach = reach_ref[...]

    @pl.loop(0, channels // 128)
    def _(lane):
        lanes = pl.ds(pl.multiple_of(lane * 128, 128), 128)
        window = glu_ref[pl.ds(top, rows + HALO), lanes].astype(jnp.float32)
        total = jnp.zeros((rows, 128), jnp.float32)
        for shift in range(8):
            held = window if shift == 0 else window[shift : shift + rows + HALO - 8]
            for offset in range(shift, HALO + 1, 8):
                lag = HALO - offset
                if lag < KERNEL:
                    moved = held[offset - shift : offset - shift + rows]
                    moved = jnp.where(reach >= lag, moved, 0.0)
                    total = total + moved * taps_ref[lag : lag + 1, lanes]
        mixed[:, lanes] = total.astype(jnp.bfloat16).astype(jnp.float32)

    wide = mixed[...]
    center = wide - jnp.mean(wide, axis=-1, keepdims=True)
    spread = jnp.mean(center * center, axis=-1, keepdims=True)
    normed = center * lax.rsqrt(spread + 1e-06) * gain_ref[...] + bias_ref[...]
    out_ref[...] = (normed * jax.nn.sigmoid(normed)).astype(jnp.bfloat16)


def mix_and_finish(glu, reach, taps, norm_gain, norm_bias):
    channels = glu.shape[1]
    count = reach.shape[0]
    rows = 64
    return pl.pallas_call(
        mix_kernel,
        grid=(count // rows,),
        out_shape=jax.ShapeDtypeStruct((count, channels), jnp.bfloat16),
        in_specs=[
            pl.BlockSpec(glu.shape, lambda i: (0, 0)),
            pl.BlockSpec((rows, 128), lambda i: (i, 0)),
            pl.BlockSpec(taps.shape, lambda i: (0, 0)),
            pl.BlockSpec((1, channels), lambda i: (0, 0)),
            pl.BlockSpec((1, channels), lambda i: (0, 0)),
        ],
        out_specs=pl.BlockSpec((rows, channels), lambda i: (i, 0)),
        scratch_shapes=[pltpu.VMEM((rows, channels), jnp.float32)],
    )(glu, reach, taps, norm_gain[None], norm_bias[None])


def per_device(tokens, documents, value_weight, gate_weight, conv_weight, norm_gain, norm_bias):
    batch, count, width = tokens.shape
    channels = value_weight.shape[1]
    lead = KERNEL - 1
    rows = tokens.reshape(batch * count, width)
    docs = documents.reshape(count)
    before_docs = passed_along(docs[count - lead :], "sp", 1)
    before_docs = jnp.where(lax.axis_index("sp") == 0, -1, before_docs)
    docs_wide = jnp.concatenate([before_docs, docs])
    reach = jnp.zeros((count,), jnp.int32)
    for lag in range(1, KERNEL):
        reach = reach + (docs_wide[lead - lag : lead - lag + count] == docs).astype(jnp.int32)
    reach = jnp.broadcast_to(reach[:, None], (count, 128))
    glu = gated_product(rows, value_weight, gate_weight)
    taps = jnp.pad(conv_weight.astype(jnp.float32), ((0, 1), (0, 0)))
    out = mix_and_finish(glu, reach, taps, norm_gain, norm_bias)
    return out.reshape(batch, count, channels)


def solution(mesh):
    return jax.shard_map(
        per_device,
        mesh=mesh,
        in_specs=(
            P("dp", "sp", None),
            P("dp", "sp"),
            P(("sp", "dp"), None),
            P(("sp", "dp"), None),
            P(),
            P(),
            P(),
        ),
        out_specs=P("dp", "sp", None),
        check_vma=False,
    )
```

time: 318 us -> 205 us (0.64)
  waiting for transfers between devices: 212 us -> 0.01 us
  Pallas kernels: 0 us -> 188 us
  other arithmetic: 56.4 us -> 4.25 us
  matrix products: 27.2 us -> 0 us
  between operations: 13.6 us -> 0.09 us
  local copies, waits for them, and re-layouts: 0.12 us -> 6.77 us
  starting transfers between devices: 8.24 us -> 4.86 us
    all_gather x2 -> x0, waiting for transfers between devices: 208 us -> none  [the longest x1 106 us: per_device(): lax.all_gather(value_weight, ('sp', 'dp'), axis=0, tiled=True)]
    pallas_call x0 -> x2, Pallas kernels: none -> 188 us  [the longest x1 162 us: gated_product(): pl.pallas_call(functools.partial(gather_kernel, side, tall), out_shape=ja...]
    convert_element_type x6 -> x0, other arithmetic: 50.3 us -> none  [the longest x1 42.9 us: per_device(): convolve(extended, docs_wide, conv_weight, count).astype(jnp.bfloat16)]
    dot_general x2 -> x0, matrix products: 27.2 us -> none  [the longest x1 13.6 us: per_device(): jnp.dot(rows, lax.all_gather(gate_weight, ('sp', 'dp'), axis=0, tiled=Tru...]
    reshape x0 -> x5, local copies, waits for them, and re-layouts: none -> 5.15 us  [the longest x2 2.48 us: gated_product(): value_weight.reshape(cut)]
    eq x8 -> x0, other arithmetic: 4.98 us -> none  [convolve(): keep = (padded_docs[:, begin:begin + count] == here)[:, :, None]]
    ppermute x2 -> x1, starting transfers between devices: 8.2 us -> 4.86 us  [passed_along(): return lax.ppermute(block, axis, route)]
  transfers between devices with their start and end apart: 4 -> 1, of which waited for: 3 -> 0; matrix products, arithmetic and copies ran while one was open for 7% -> 5% of each run, Pallas kernels for 0% -> 79%
where the time goes in v1:
time: 205 us; the launch traced here: 204 us
  Pallas kernels  188 us (92%)
  local copies, waits for them, and re-layouts  6.77 us (3%)
  starting transfers between devices  4.86 us (2%)
  other arithmetic  4.25 us (2%)
    pallas_call x1, Pallas kernels, gated_product(): pl.pallas_call(functools.partial(gather_kernel, side, tall), out_shape=ja...  162 us
    pallas_call x1, Pallas kernels, mix_and_finish(): pl.pallas_call(mix_kernel, grid=(count // rows,), out_shape=jax.ShapeDtyp...  26.3 us
    ppermute x1, starting transfers between devices, passed_along(): return lax.ppermute(block, axis, route)  4.86 us
  transfers between devices with their start and end apart: 1, of which 0 were waited for; matrix products, arithmetic and copies ran while one was open for 5% of the time, Pallas kernels for 79%

profile of v1, /device:TPU:0, one launch (start us, length us, event | category | flops | bytes accessed | tf_op | source)
XLA Modules:
  0.0 204.5 jit_solution(9567032164387596264)
XLA Ops:
  0.0 0.0 copy-start
  0.0 0.8 slice_bitcast_fusion
  0.8 4.9 %collective-permute-start = (s32[30]{0:T(128)S(1)}, s32[30]{0:T(128)S(1)}, u32[]{:S(2)}, u32[]{:S(2)}) collective-permute-start(s32[30]{0:T(128)S(1)} %slice_bitcast_fusion), channel_id=1, source_target_pairs={{0,4},{4,8},{8,12},{12,16},{16,20},{20,24},{24,28},{1,5},{5,9},{9,... | collective-permute-start | bytes 368 | tf_op jit(solution)/shard_map/ppermute | solution.py:276
  5.7 1.6 pad_convert_fusion.taps_ref
  7.3 1.4 reshape.21
  8.7 1.1 copy.8
  9.8 0.0 copy-done
  9.8 0.4 reshape.22
  10.2 1.1 copy.9
  11.2 2.4 %maximum_bitcast_fusion = bf16[2,4,128,2,2,128]{5,4,3,2,1,0:T(2,128)(2,1)S(1)} fusion(bf16[128,2,4,2,1,128]{5,4,3,0,2,1:T(2,128)(2,1)S(1)} %copy.9, bf16[128,2,4,2,1,128]{5,4,3,0,2,1:T(2,128)(2,1)S(1)} %copy.8), kind=kLoop, calls=%fused_computation | loop fusion | flops 2097152 | bytes 2097152 | tf_op jit(solution)/shard_map/transpose | solution.py:251
  13.7 1.2 reshape.23.own_hbm
  14.9 0.0 copy-start.1
  14.9 162.2 %shard_map.73.glu_ref = bf16[544,2048]{1,0:T(8,128)(2,1)} custom-call(bf16[512,4096]{1,0:T(8,128)(2,1)} %bitcast.9, bf16[2,4,128,512]{3,2,1,0:T(8,128)(2,1)} %reshape.23.own_hbm), custom_call_target="tpu_custom_call" | custom-call | tf_op jit(solution)/shard_map/pallas_call | solution.py:253
  177.1 0.0 collective-permute-done
  177.1 0.0 copy-done.1
  177.1 0.1 pad_add_fusion
  177.2 0.1 convert_add_fusion
  177.3 0.8 broadcast_in_dim.17.reach_ref
  178.2 26.3 %shard_map.74 = bf16[512,2048]{1,0:T(8,128)(2,1)} custom-call(bf16[544,2048]{1,0:T(8,128)(2,1)} %shard_map.73.glu_ref, s32[512,128]{1,0:T(8,128)} %broadcast_in_dim.17.reach_ref, f32[32,2048]{1,0:T(8,128)} %pad_convert_fusion.taps_ref, f32[1,2048]{1,0:T(1,128)} %bitcast.10, f32[1,2048]{1,0:T(1,128)} %bitcast.11), custom_call_target="tpu_custom_call" | custom-call | tf_op jit(solution)/shard_map/pallas_call | solution.py:310
  (1 shorter events, 0.0 us)
Async XLA Ops:
  0.0 9.8 %copy-start = (bf16[128,2048]{1,0:T(8,128)(2,1)S(1)}, bf16[128,2048]{1,0:T(8,128)(2,1)}, u32[]{:S(2)}) copy-start(bf16[128,2048]{1,0:T(8,128)(2,1)} %param.10) | copy-start | bytes 1572868
  0.8 176.3 %collective-permute-start = (s32[30]{0:T(128)S(1)}, s32[30]{0:T(128)S(1)}, u32[]{:S(2)}, u32[]{:S(2)}) collective-permute-start(s32[30]{0:T(128)S(1)} %slice_bitcast_fusion), channel_id=1, source_target_pairs={{0,4},{4,8},{8,12},{12,16},{16,20},{20,24},{24,28},{1,5},{5,9},{9,... | collective-permute-start | bytes 368 | tf_op jit(solution)/shard_map/ppermute | solution.py:276
  14.9 162.2 %copy-start.1 = (s32[1,512]{1,0:T(1,128)S(1)}, s32[1,512]{1,0:T(1,128)}, u32[]{:S(2)}) copy-start(s32[1,512]{1,0:T(1,128)} %param.8) | copy-start | bytes 6148
